TPU v7x, 32 devices: a whole 2x2x4 slice. The times are simulated.
32 devices in a mesh: sp: 8 (over z, x), tp: 4 (over y, core).
Axes of the slice: x: 2, y: 2, z: 4, core: 2. Of those that a mesh axis runs over, the one named last changes fastest.
Arguments:
- residual: bfloat16 [4096, 2048], P('sp', 'tp'), may hold values from -64 to 64
- gains: float32 [2, 2, 2048], replicated, may hold values from 0.1 to 1.9
- w_query: bfloat16 [2, 2048, 2048], P(None, None, 'tp'), may hold values from -0.125 to 0.125
- w_key: bfloat16 [2, 2048, 2048], P(None, None, 'tp'), may hold values from -0.125 to 0.125
- w_value: bfloat16 [2, 2048, 2048], P(None, None, 'tp'), may hold values from -0.125 to 0.125
- w_out: bfloat16 [2, 2048, 2048], P(None, None, 'tp'), may hold values from -1 to 1
- rel_bias: float32 [2, 32, 257], P(None, 'tp'), may hold values from -6 to 300
Outputs:
- encoded: bfloat16 [4096, 2048], P('sp', 'tp')
All inputs are finite; a program needn't handle non-finite values.
Results may differ from a plain program's by a relative error of at most 0.0058.
Values may be sent and summed in bfloat16 or wider, within the bound.
A program may use at most 128 MiB of HBM per device.

v0:
```python
import functools

import jax
import jax.numpy as jnp
from jax import lax
from jax.experimental import pallas as pl
from jax.experimental.pallas import tpu as pltpu
from jax.sharding import PartitionSpec as P

HEAD = 64
SEG = 64
LEFT = 8
MAXREL = 128
BLOCK = 128
EPS = 1e-06
LOG2E = 1.4426950408889634
NEG = -1e30
MESH = pl.DeviceIdType.MESH
F32 = jnp.float32
BF16 = jnp.bfloat16


def remote(src, dst, send_sem, recv_sem, where):
    return pltpu.make_async_remote_copy(
        src_ref=src,
        dst_ref=dst,
        send_sem=send_sem,
        recv_sem=recv_sem,
        device_id=where,
        device_id_type=MESH,
    )


def kernel(
    tp,
    sp_count,
    res_ref,
    gains_ref,
    bias_ref,
    wq_ref,
    wk_ref,
    wv_ref,
    wo_ref,
    out_ref,
    wbuf,
    gather,
    kbuf,
    vbuf,
    qbuf,
    branch,
    toeplitz,
    sums,
    w_sem,
    g_send,
    g_recv,
    f_send,
    h_send,
    h_recv,
    s_send,
    s_recv,
):
    layers = wbuf.shape[0]
    tokens, cols = res_ref.shape
    width = cols * tp
    chunks = tokens // BLOCK
    pairs = cols // 128
    reach = LEFT * SEG
    blocks = reach // BLOCK
    me = lax.axis_index("tp")
    sp = lax.axis_index("sp")
    core = lax.rem(me, 2)
    sibling = me + 1 - 2 * core
    ychips = tp // 2

    weights = (wq_ref, wk_ref, wv_ref, wo_ref)

    def weight_copy(l, k):
        return pltpu.make_async_copy(weights[k].at[l], wbuf.at[l, k], w_sem.at[l, k])

    for l in range(layers):
        for k in range(4):
            weight_copy(l, k).start()

    barrier = pltpu.get_barrier_semaphore()
    for k in range(1, tp):
        pl.semaphore_signal(
            barrier, inc=1, device_id={"tp": lax.rem(me + k, tp)}, device_id_type=MESH
        )
    for k in (1, sp_count - 1):
        pl.semaphore_signal(
            barrier, inc=1, device_id={"sp": lax.rem(sp + k, sp_count)}, device_id_type=MESH
        )
    pl.semaphore_wait(barrier, tp + 1)

    def rows_of(c):
        return pl.ds(pl.multiple_of(c * BLOCK, BLOCK), BLOCK)

    def block_of(kind, l, c, slot):
        return gather.at[kind, l, slot, rows_of(c)]

    def direct(kind, l, c, peer, source):
        ref = block_of(kind, l, c, source)
        return remote(
            ref, ref, g_send.at[kind, c, peer], g_recv.at[kind, l, c, source], {"tp": peer}
        )

    def forward(kind, l, c, source):
        ref = block_of(kind, l, c, source)
        return remote(
            ref, ref, f_send.at[kind, c, source], g_recv.at[kind, l, c, source], {"tp": sibling}
        )

    def spread(kind, l, c):
        for k in range(1, ychips):
            direct(kind, l, c, lax.rem(me + 2 * k, tp), me).start()
        direct(kind, l, c, sibling, me).start()

    def relay(kind, l, c):
        for k in range(1, ychips):
            source = lax.rem(me + 2 * k, tp)
            direct(kind, l, c, source, source).wait_recv()
            forward(kind, l, c, source).start()

    def arrive(kind, l, c):
        direct(kind, l, c, sibling, sibling).wait_recv()
        for k in range(1, ychips):
            source = lax.rem(sibling + 2 * k, tp)
            direct(kind, l, c, sibling, source).wait_recv()
        for k in range(1, ychips):
            forward(kind, l, c, lax.rem(me + 2 * k, tp)).wait_send()
            direct(kind, l, c, lax.rem(me + 2 * k, tp), me).wait_send()
        direct(kind, l, c, sibling, me).wait_send()

    def halo(l, c, which):
        buf = (kbuf, vbuf)[which]
        return remote(
            buf.at[l, rows_of(c + blocks)],
            buf.at[l, rows_of(c)],
            h_send.at[c, which],
            h_recv.at[l, c, which],
            {"sp": lax.rem(sp + 1, sp_count)},
        )

    def sum_copy(l, c, peer, source):
        ref = sums.at[l, c, source]
        return remote(ref, ref, s_send.at[peer], s_recv.at[l, c, source], {"tp": peer})

    gather[0, 0, me] = res_ref[...]
    for t in range(chunks):
        spread(0, 0, chunks - 1 - t)

    @pl.when(sp == 0)
    def _():
        for l in range(layers):
            kbuf[l, :reach] = jnp.zeros((reach, cols), BF16)
            vbuf[l, :reach] = jnp.zeros((reach, cols), BF16)

    row = lax.broadcasted_iota(jnp.int32, (BLOCK, BLOCK), 0)
    col = lax.broadcasted_iota(jnp.int32, (BLOCK, BLOCK), 1)
    low = col < HEAD
    early = jnp.where((row >= SEG) & (col < SEG), NEG, 0.0).astype(F32)
    late = jnp.where((row < SEG) & (col >= SEG), NEG, 0.0).astype(F32)

    def project(l, c):
        arrive(0, l, c)
        parts = [gather[0, l, j, rows_of(c)].astype(F32) for j in range(tp)]
        total = sum(jnp.sum(p * p, axis=1, keepdims=True) for p in parts)
        inv = lax.rsqrt(total / width + EPS)
        gain = gains_ref[l, 0:1, :]
        normed = jnp.concatenate(
            [
                (p * inv * gain[:, j * cols : (j + 1) * cols]).astype(BF16)
                for j, p in enumerate(parts)
            ],
            axis=1,
        )
        own = rows_of(c + blocks)
        kbuf[l, own] = jnp.dot(normed, wbuf[l, 1], preferred_element_type=F32).astype(BF16)
        vbuf[l, own] = jnp.dot(normed, wbuf[l, 2], preferred_element_type=F32).astype(BF16)

        @pl.when(sp < sp_count - 1)
        def _():
            halo(l, c, 0).start()
            halo(l, c, 1).start()

        query = jnp.dot(normed, wbuf[l, 0], preferred_element_type=F32)
        qbuf[rows_of(c)] = (query * (LOG2E * HEAD**-0.5)).astype(BF16)

    def attention(l, c):
        @pl.when(sp > 0)
        def _():
            halo(l, c, 0).wait_recv()
            halo(l, c, 1).wait_recv()

        @pl.when(sp < sp_count - 1)
        def _():
            halo(l, c, 0).wait_send()
            halo(l, c, 1).wait_send()

        window = pl.ds(pl.multiple_of(c * BLOCK, BLOCK), reach + BLOCK)
        closed = [
            jnp.where((sp == 0) & (c + i < blocks), NEG, 0.0).astype(F32) for i in range(blocks)
        ]

        for pair in range(pairs):
            lanes = slice(pair * 128, (pair + 1) * 128)
            query = qbuf[rows_of(c), lanes]
            keys = kbuf[l, window, lanes]
            values = vbuf[l, window, lanes]
            halves = []
            for half in range(2):
                mine = low if half == 0 else ~low
                masked = jnp.where(mine, query.astype(F32), 0.0).astype(BF16)
                scores = lax.dot_general(
                    masked, keys, (((1,), (1,)), ((), ())), preferred_element_type=F32
                )
                tiles = []
                for i in range(blocks + 1):
                    tile = scores[:, i * BLOCK : (i + 1) * BLOCK]
                    if i == 0:
                        tile = tile + early
                    if i >= blocks - 1:
                        at = (i - blocks + 1) * BLOCK
                        tile = tile + toeplitz[l, 2 * pair + half, :, at : at + BLOCK]
                    if i < blocks:
                        tile = tile + closed[i]
                    tiles.append(tile)
                top = functools.reduce(jnp.maximum, tiles)
                top = jnp.max(top, axis=1, keepdims=True)
                tiles = [jnp.exp2(tile - top) for tile in tiles]
                total = jnp.sum(functools.reduce(jnp.add, tiles), axis=1, keepdims=True)
                raw = jnp.concatenate([tile.astype(BF16) for tile in tiles], axis=1)
                mixed = jnp.dot(raw, values, preferred_element_type=F32)
                halves.append(mixed / total)
            gather[1, l, me, rows_of(c), lanes] = jnp.where(low, halves[0], halves[1]).astype(BF16)
        spread(1, l, c)

    def out_project(l, c):
        arrive(1, l, c)
        whole = jnp.concatenate([gather[1, l, j, rows_of(c)] for j in range(tp)], axis=1)
        value = jnp.dot(whole, wbuf[l, 3], preferred_element_type=F32)
        branch[rows_of(c)] = value
        square = jnp.sum(value * value, axis=1, keepdims=True)
        sums[l, c, me] = jnp.broadcast_to(square, (BLOCK, BLOCK)).T[:8]
        for k in range(1, tp):
            sum_copy(l, c, lax.rem(me + k, tp), me).start()

    def finish(l, c):
        for k in range(1, tp):
            peer = lax.rem(me + k, tp)
            sum_copy(l, c, peer, peer).wait_recv()
            sum_copy(l, c, peer, me).wait_send()
        total = functools.reduce(jnp.add, [sums[l, c, j] for j in range(tp)])
        inv = lax.rsqrt(total / width + EPS)
        inv = jnp.broadcast_to(inv[0:1], (BLOCK, BLOCK)).T[:, 0:1]
        gain = gains_ref[l, 1:2, pl.ds(pl.multiple_of(me * cols, 128), cols)]
        new = gather[0, l, me, rows_of(c)].astype(F32) + branch[rows_of(c)] * inv * gain
        new = new.astype(BF16)

        @pl.when(l == layers - 1)
        def _():
            out_ref[rows_of(c)] = new

        @pl.when(l < layers - 1)
        def _():
            later = jnp.minimum(l + 1, layers - 1)
            gather[0, later, me, rows_of(c)] = new
            spread(0, later, c)

    def tables(l, carry):
        far = bias_ref[l, :, 2 * MAXREL :]
        near = (bias_ref[l, :, : 2 * MAXREL] - far) * LOG2E
        for h in range(2 * pairs):
            line = jnp.concatenate([jnp.zeros((1, BLOCK), F32), near[h : h + 1]], axis=1)
            line = jnp.broadcast_to(line, (2 * BLOCK, 3 * BLOCK))
            skewed = pltpu.roll(line, 0, 1, stride=1, stride_axis=0)
            toeplitz[l, h, :, :BLOCK] = skewed[:BLOCK, :BLOCK].T
            toeplitz[l, h, :, BLOCK:] = skewed[BLOCK:, :BLOCK].T + late
        return carry

    lax.fori_loop(0, layers, tables, 0)

    for k in range(3):
        weight_copy(0, k).wait()

    def enter(t, carry):
        @pl.when(t < chunks)
        def _():
            relay(0, 0, chunks - 1 - t)

        @pl.when(t >= 1)
        def _():
            project(0, chunks - t)

        return carry

    lax.fori_loop(0, chunks + 1, enter, 0)
    weight_copy(0, 3).wait()

    def layer(l, carry):
        later = jnp.minimum(l + 1, layers - 1)
        more = l < layers - 1

        def stage(t, lag, needed=True):
            return (t >= lag) & (t < lag + chunks) & needed

        def step(t, carry):
            def at(lag):
                return chunks - 1 - t + lag

            @pl.when(stage(t, 0))
            def _():
                attention(l, at(0))

            @pl.when(stage(t, 1))
            def _():
                relay(1, l, at(1))

            @pl.when(stage(t, 2))
            def _():
                out_project(l, at(2))

            @pl.when(stage(t, 3))
            def _():
                finish(l, at(3))

            @pl.when((t == 4) & more)
            def _():
                for k in range(4):
                    weight_copy(later, k).wait()

            @pl.when(stage(t, 4, more))
            def _():
                relay(0, later, at(4))

            @pl.when(stage(t, 5, more))
            def _():
                project(later, at(5))

            return carry

        lax.fori_loop(0, chunks + 5, step, 0)
        return carry

    lax.fori_loop(0, layers, layer, 0)


def on_device(tp, sp_count, residual, gains, w_query, w_key, w_value, w_out, rel_bias):
    tokens, cols = residual.shape
    layers, width, _ = w_query.shape
    chunks = tokens // BLOCK
    reach = LEFT * SEG
    heads = cols // HEAD
    vmem = pl.BlockSpec(memory_space=pltpu.VMEM)
    hbm = pl.BlockSpec(memory_space=pl.ANY)
    dma = pltpu.SemaphoreType.DMA
    return pl.pallas_call(
        functools.partial(kernel, tp, sp_count),
        out_shape=jax.ShapeDtypeStruct((tokens, cols), BF16),
        in_specs=[vmem, vmem, vmem, hbm, hbm, hbm, hbm],
        out_specs=vmem,
        scratch_shapes=[
            pltpu.VMEM((layers, 4, width, cols), BF16),
            pltpu.VMEM((2, layers, tp, tokens, cols), BF16),
            pltpu.VMEM((layers, reach + tokens, cols), BF16),
            pltpu.VMEM((layers, reach + tokens, cols), BF16),
            pltpu.VMEM((tokens, cols), BF16),
            pltpu.VMEM((tokens, cols), F32),
            pltpu.VMEM((layers, heads, BLOCK, 2 * BLOCK), F32),
            pltpu.VMEM((layers, chunks, tp, 8, BLOCK), F32),
            dma((layers, 4)),
            dma((2, chunks, tp)),
            dma((2, layers, chunks, tp)),
            dma((2, chunks, tp)),
            dma((chunks, 2)),
            dma((layers, chunks, 2)),
            dma((tp,)),
            dma((layers, chunks, tp)),
        ],
        compiler_params=pltpu.CompilerParams(
            collective_id=0, has_side_effects=True, vmem_limit_bytes=58 * 2**20
        ),
    )(residual, gains, rel_bias, w_query, w_key, w_value, w_out)


def solution(mesh):
    return jax.shard_map(
        functools.partial(on_device, mesh.shape["tp"], mesh.shape["sp"]),
        mesh=mesh,
        in_specs=(
            P("sp", "tp"),
            P(),
            P(None, None, "tp"),
            P(None, None, "tp"),
            P(None, None, "tp"),
            P(None, None, "tp"),
            P(None, "tp", None),
        ),
        out_specs=P("sp", "tp"),
        check_vma=False,
    )
```

profile of v0, /device:TPU:9, one launch (start us, length us, event | category | flops | bytes accessed | tf_op | source)
XLA Modules:
  0.0 90.7 jit_solution(137833266812936910)
XLA Ops:
  0.0 88.8 %shard_map.73 = bf16[512,512]{1,0:T(8,128)(2,1)} custom-call(bf16[512,512]{1,0:T(8,128)(2,1)} %res_ref.1, f32[2,2,2048]{2,1,0:T(2,128)} %gains_ref.1, f32[2,8,257]{2,1,0:T(8,128)} %bias_ref.1, bf16[2,2048,512]{2,1,0:T(8,128)(2,1)} %wq_ref.1, bf16[2,2048,512]{2,1,0:T(8,128)(2,1)} %wk_ref.1, bf16[2,2048,512]{2,1,0:T(8,128)(2,1)} %wv_ref.1, ...), custom_call_target="tpu_custom_call" | custom-call | tf_op jit(solution)/shard_map/pallas_call | solution.py:357
  88.8 1.9 %copy.9 = bf16[512,512]{1,0:T(8,128)(2,1)} copy(bf16[512,512]{1,0:T(8,128)(2,1)} %shard_map.73) | data formatting | bytes 1048576
where the time goes:
time: 90.9 us; the launch traced here: 90.7 us
  Pallas kernels  88.8 us (98%)
  local copies, waits for them, and re-layouts  1.87 us (2%)
    pallas_call x1, Pallas kernels, on_device(): pl.pallas_call(functools.partial(kernel, tp, sp_count), out_shape=jax.Sha...  88.8 us
    unnamed x1, local copies, waits for them, and re-layouts  1.87 us

commit v1 on v0

v1 whole, which is shorter than its diff:
```python
import functools

import jax
import jax.numpy as jnp
from jax import lax
from jax.experimental import pallas as pl
from jax.experimental.pallas import tpu as pltpu
from jax.sharding import PartitionSpec as P

HEAD = 64
SEG = 64
LEFT = 8
MAXREL = 128
BLOCK = 128
EPS = 1e-06
LOG2E = 1.4426950408889634
NEG = -1e30
SENT = 1
MESH = pl.DeviceIdType.MESH
F32 = jnp.float32
BF16 = jnp.bfloat16


def remote(src, dst, send_sem, recv_sem, where):
    return pltpu.make_async_remote_copy(
        src_ref=src,
        dst_ref=dst,
        send_sem=send_sem,
        recv_sem=recv_sem,
        device_id=where,
        device_id_type=MESH,
    )


def kernel(
    tp,
    sp_count,
    res_ref,
    gains_hbm,
    bias_hbm,
    wq_ref,
    wk_ref,
    wv_ref,
    wo_ref,
    out_ref,
    wbuf,
    gather,
    before,
    kbuf,
    vbuf,
    qbuf,
    branch,
    toeplitz,
    sums,
    gains_ref,
    bias_ref,
    final,
    w_sem,
    io_sem,
    g_send,
    g_recv,
    f_send,
    b_send,
    b_recv,
    bf_send,
    h_send,
    h_recv,
    s_send,
    s_recv,
):
    layers = wbuf.shape[0]
    tokens, cols = res_ref.shape
    width = cols * tp
    chunks = tokens // BLOCK
    pairs = cols // 128
    reach = LEFT * SEG
    blocks = reach // BLOCK
    me = lax.axis_index("tp")
    sp = lax.axis_index("sp")
    core = lax.rem(me, 2)
    sibling = me + 1 - 2 * core
    ychips = tp // 2
    first = sp == 0
    last = sp == sp_count - 1

    weights = (wq_ref, wk_ref, wv_ref, wo_ref)

    def weight_copy(l, k):
        return pltpu.make_async_copy(weights[k].at[l], wbuf.at[l, k], w_sem.at[l, k])

    def rows_of(c):
        return pl.ds(pl.multiple_of(c * BLOCK, BLOCK), BLOCK)

    def res_copy(c):
        return pltpu.make_async_copy(
            res_ref.at[rows_of(c)], gather.at[0, 0, me, rows_of(c)], io_sem.at[c]
        )

    def out_copy(c):
        return pltpu.make_async_copy(final.at[rows_of(c)], out_ref.at[rows_of(c)], io_sem.at[c])

    gains_copy = pltpu.make_async_copy(gains_hbm, gains_ref, io_sem.at[chunks])
    bias_copy = pltpu.make_async_copy(bias_hbm, bias_ref, io_sem.at[chunks + 1])

    for c in reversed(range(chunks)):
        res_copy(c).start()
    bias_copy.start()
    gains_copy.start()
    for k in (1, 2, 0):
        weight_copy(0, k).start()

    barrier = pltpu.get_barrier_semaphore()
    for k in range(1, tp):
        pl.semaphore_signal(
            barrier, inc=1, device_id={"tp": lax.rem(me + k, tp)}, device_id_type=MESH
        )
    for k in (1, sp_count - 1):
        pl.semaphore_signal(
            barrier, inc=1, device_id={"sp": lax.rem(sp + k, sp_count)}, device_id_type=MESH
        )
    pl.semaphore_wait(barrier, tp + 1)

    def block_of(kind, l, c, slot):
        return gather.at[kind, l, slot, rows_of(c)]

    def direct(kind, l, c, peer, source):
        ref = block_of(kind, l, c, source)
        return remote(ref, ref, g_send.at[kind, c, peer], g_recv.at[kind, c, source], {"tp": peer})

    def forward(kind, l, c, source):
        ref = block_of(kind, l, c, source)
        return remote(
            ref, ref, f_send.at[kind, c, source // 2], g_recv.at[kind, c, source], {"tp": sibling}
        )

    def others(base):
        return [lax.rem(base + 2 * k, tp) for k in range(1, ychips)]

    def spread(kind, l, c):
        for peer in others(me):
            direct(kind, l, c, peer, me).start()
        direct(kind, l, c, sibling, me).start()

    def relay(kind, l, c):
        for source in others(me):
            direct(kind, l, c, source, source).wait_recv()
            forward(kind, l, c, source).start()

    def arrive(kind, l, c):
        direct(kind, l, c, sibling, sibling).wait_recv()
        for source in others(sibling):
            direct(kind, l, c, sibling, source).wait_recv()
        for source in others(me):
            forward(kind, l, c, source).wait_send()
            direct(kind, l, c, source, me).wait_send()
        direct(kind, l, c, sibling, me).wait_send()

    def pass_on(l, c, source):
        return remote(
            block_of(0, l, c, source),
            before.at[l, source, rows_of(c - SENT)],
            b_send.at[c - SENT, source // 2],
            b_recv.at[l, c - SENT, source],
            {"sp": lax.rem(sp + 1, sp_count)},
        )

    def pass_across(l, c, source):
        ref = before.at[l, source, rows_of(c - SENT)]
        return remote(
            ref,
            ref,
            bf_send.at[c - SENT, source // 2],
            b_recv.at[l, c - SENT, source],
            {"tp": sibling},
        )

    def relay_stream(l, c):
        relay(0, l, c)

        @pl.when((c >= SENT) & ~last)
        def _():
            for source in others(me):
                pass_on(l, c, source).start()

        @pl.when((l == 0) & (c == chunks - 1) & ~last)
        def _():
            for held in reversed(range(SENT, chunks - 2)):
                pass_on(0, held, me).start()

    def update(l, parts):
        old, branches = parts
        branches = [part.astype(F32) for part in branches]
        total = sum(jnp.sum(part * part, axis=1, keepdims=True) for part in branches)
        inv = lax.rsqrt(total / width + EPS)
        gain = gains_ref[l - 1, 1:2, :]
        return [
            (part.astype(F32) + b * inv * gain[:, j * cols : (j + 1) * cols]).astype(BF16)
            for j, (part, b) in enumerate(zip(old, branches))
        ]

    def relay_before(l, c, sources):
        @pl.when(~first)
        def _():
            for source in sources:
                pass_on(l, c, source).wait_recv()
                pass_across(l, c, source).start()

    def halo(l, c, which):
        if which == 0:
            src, dst = kbuf.at[l, rows_of(c + blocks)], kbuf.at[l, rows_of(c)]
        else:
            src, dst = vbuf.at[l, c + blocks], vbuf.at[l, c]
        return remote(
            src,
            dst,
            h_send.at[c, which],
            h_recv.at[l, c, which],
            {"sp": lax.rem(sp + 1, sp_count)},
        )

    def sum_copy(c, peer, source):
        ref = sums.at[c, source]
        return remote(ref, ref, s_send.at[c, peer], s_recv.at[c, source], {"tp": peer})

    for c in reversed(range(chunks)):
        res_copy(c).wait()
        spread(0, 0, c)
        if c >= max(SENT, chunks - 2):

            @pl.when(~last)
            def _():
                pass_on(0, c, me).start()

    @pl.when(first)
    def _():
        for l in range(layers):
            kbuf[l, :reach] = jnp.zeros((reach, cols), BF16)
            vbuf[l, :blocks] = jnp.zeros((blocks, cols, BLOCK), BF16)

    row = lax.broadcasted_iota(jnp.int32, (BLOCK, BLOCK), 0)
    col = lax.broadcasted_iota(jnp.int32, (BLOCK, BLOCK), 1)
    low = col < HEAD
    late = jnp.where((row >= SEG) & (col < SEG), NEG, 0.0).astype(F32)
    place = lax.broadcasted_iota(jnp.int32, (1, 2 * BLOCK), 1)
    early = jnp.where(lax.rem(place, BLOCK) >= SEG, NEG, 0.0).astype(F32)

    def scaled_and_inv(l, parts):
        parts = [part.astype(F32) for part in parts]
        gain = gains_ref[l, 0:1, :]
        scaled = jnp.concatenate(
            [
                (part * gain[:, j * cols : (j + 1) * cols]).astype(BF16)
                for j, part in enumerate(parts)
            ],
            axis=1,
        )
        total = sum(jnp.sum(part * part, axis=1, keepdims=True) for part in parts)
        return scaled, lax.rsqrt(total / width + EPS)

    def store_keys_values(l, slot, scaled, inv):
        key = jnp.dot(scaled, wbuf[l, 1], preferred_element_type=F32)
        kbuf[l, rows_of(slot)] = (key * inv).astype(BF16)
        value = jnp.dot(scaled, wbuf[l, 2], preferred_element_type=F32)
        vbuf[l, slot] = (value * inv).T.astype(BF16)

    def project(l, c):
        arrive(0, l, c)
        rows = rows_of(c)

        @pl.when(l > 0)
        def _():
            own = ([gather[0, k, j, rows] for j in range(tp)] for k in (0, l))
            for j, part in enumerate(update(l, own)):
                gather[0, 0, j, rows] = part

        scaled, inv = scaled_and_inv(l, [gather[0, 0, j, rows] for j in range(tp)])
        query = jnp.dot(scaled, wbuf[l, 0], preferred_element_type=F32)
        qbuf[rows_of(c)] = (query * (inv * (LOG2E * HEAD**-0.5))).astype(BF16)
        store_keys_values(l, c + blocks, scaled, inv)

        @pl.when((c < SENT) & ~last)
        def _():
            halo(l, c, 0).start()
            halo(l, c, 1).start()

    def project_before(l, c):
        @pl.when(~first)
        def _():
            for source in [sibling] + others(sibling):
                pass_across(l, c, source).wait_recv()
            for source in [me] + others(me):
                pass_across(l, c, source).wait_send()
            rows = rows_of(c - SENT)

            @pl.when(l > 0)
            def _():
                halo_parts = ([before[k, j, rows] for j in range(tp)] for k in (0, l))
                for j, part in enumerate(update(l, halo_parts)):
                    before[0, j, rows] = part

            scaled, inv = scaled_and_inv(l, [before[0, j, rows] for j in range(tp)])
            store_keys_values(l, c, scaled, inv)

    def attention(l, c):
        @pl.when((c < SENT) & ~first)
        def _():
            halo(l, c, 0).wait_recv()
            halo(l, c, 1).wait_recv()

        window = pl.ds(pl.multiple_of(c * BLOCK, BLOCK), reach + BLOCK)
        closed = [
            jnp.where(first & (c + i < blocks), NEG, 0.0).astype(F32) for i in range(blocks)
        ]

        def score(pair):
            lanes = slice(pair * 128, (pair + 1) * 128)
            query = qbuf[rows_of(c), lanes]
            zero = jnp.zeros_like(query)
            both = jnp.concatenate(
                [jnp.where(low, query, zero), jnp.where(low, zero, query)], axis=0
            )
            scores = lax.dot_general(
                kbuf[l, window, lanes],
                both,
                (((1,), (1,)), ((), ())),
                preferred_element_type=F32,
            )
            tiles = []
            tops = []
            for i in range(blocks + 1):
                tile = scores[i * BLOCK : (i + 1) * BLOCK]
                if i == 0:
                    tile = jnp.concatenate([tile[:SEG] + early, tile[SEG:]], axis=0)
                if i >= blocks - 1:
                    tile = tile + toeplitz[l, pair, i - blocks + 1]
                top = jnp.max(tile.reshape(BLOCK // 8, 8, 2 * BLOCK), axis=0)
                if i < blocks:
                    top = top + closed[i]
                tiles.append(tile)
                tops.append(top)
            return tiles, jnp.max(functools.reduce(jnp.maximum, tops), axis=0, keepdims=True)

        def mix(pair, tiles, top):
            lanes = slice(pair * 128, (pair + 1) * 128)
            raw = []
            parts = []
            for i in range(blocks + 1):
                tile = jnp.exp2(tiles[i] - (top - closed[i] if i < blocks else top))
                parts.append(jnp.sum(tile.reshape(BLOCK // 8, 8, 2 * BLOCK), axis=0))
                raw.append(tile.astype(BF16))
            total = jnp.sum(functools.reduce(jnp.add, parts), axis=0, keepdims=True)
            values = jnp.concatenate([vbuf[l, c + i, lanes] for i in range(blocks + 1)], axis=1)
            mixed = jnp.dot(values, jnp.concatenate(raw, axis=0), preferred_element_type=F32)
            mixed = mixed * (1.0 / total)
            mixed = jnp.concatenate([mixed[:HEAD, :BLOCK], mixed[HEAD:, BLOCK:]], axis=0)
            gather[1, l, me, rows_of(c), lanes] = mixed.T.astype(BF16)

        held = [score(pair) for pair in range(pairs)]
        for pair in range(pairs):
            mix(pair, *held[pair])
        spread(1, l, c)

    def out_project(l, c):
        arrive(1, l, c)
        whole = jnp.concatenate([gather[1, l, j, rows_of(c)] for j in range(tp)], axis=1)
        value = jnp.dot(whole, wbuf[l, 3], preferred_element_type=F32)

        @pl.when(l < layers - 1)
        def _():
            later = jnp.minimum(l + 1, layers - 1)
            gather[0, later, me, rows_of(c)] = value.astype(BF16)
            spread(0, later, c)

            @pl.when((c >= SENT) & ~last)
            def _():
                pass_on(later, c, me).start()

        @pl.when(l == layers - 1)
        def _():
            branch[rows_of(c)] = value
            square = jnp.sum(value * value, axis=1, keepdims=True)
            sums[c, me] = jnp.broadcast_to(square, (BLOCK, BLOCK)).T[:8]
            for k in range(1, tp):
                sum_copy(c, lax.rem(me + k, tp), me).start()

    def finish(c):
        for k in range(1, tp):
            peer = lax.rem(me + k, tp)
            sum_copy(c, peer, peer).wait_recv()
            sum_copy(c, peer, me).wait_send()
        total = functools.reduce(jnp.add, [sums[c, j] for j in range(tp)])
        inv = lax.rsqrt(total / width + EPS)
        inv = jnp.broadcast_to(inv[0:1], (BLOCK, BLOCK)).T[:, 0:1]
        gain = gains_ref[layers - 1, 1:2, pl.ds(pl.multiple_of(me * cols, 128), cols)]
        new = gather[0, 0, me, rows_of(c)].astype(F32) + branch[rows_of(c)] * inv * gain
        final[rows_of(c)] = new.astype(BF16)
        out_copy(c).start()

    def passed_on(l):
        @pl.when(~last)
        def _():
            for c in range(chunks):
                if c < SENT:
                    halo(l, c, 0).wait_send()
                    halo(l, c, 1).wait_send()
                else:
                    for source in [me] + others(me):
                        pass_on(l, c, source).wait_send()

    def tables(l, carry):
        far = bias_ref[l, :, 2 * MAXREL :]
        near = (bias_ref[l, :, : 2 * MAXREL] - far) * LOG2E
        for h in range(2 * pairs):
            line = jnp.concatenate([jnp.zeros((1, BLOCK), F32), near[h : h + 1]], axis=1)
            line = jnp.broadcast_to(line, (2 * BLOCK, 3 * BLOCK))
            skewed = pltpu.roll(line, 0, 1, stride=1, stride_axis=0)
            at = slice(h % 2 * BLOCK, (h % 2 + 1) * BLOCK)
            toeplitz[l, h // 2, 0, :, at] = skewed[:BLOCK, :BLOCK]
            toeplitz[l, h // 2, 1, :, at] = skewed[BLOCK:, :BLOCK] + late
        return carry

    bias_copy.wait()
    lax.fori_loop(0, layers, tables, 0)
    gains_copy.wait()

    period = 2 * chunks + 1

    def step(g, carry):
        l = jnp.minimum(g // period, layers - 1)
        t = g - l * period

        def stage(lag, count=chunks):
            return (t >= lag) & (t < lag + count)

        def at(lag):
            return chunks - 1 - t + lag

        @pl.when(stage(0))
        def _():
            relay_stream(l, at(0))

        @pl.when(stage(1, chunks - SENT))
        def _():
            relay_before(l, at(1), [me])

        @pl.when(stage(chunks - 1, chunks - SENT))
        def _():
            project_before(l, at(chunks - 1))

        @pl.when(g == 0)
        def _():
            for k in (1, 2, 0):
                weight_copy(0, k).wait()
            weight_copy(0, 3).start()

        @pl.when((t == 0) & (l > 0))
        def _():
            for k in (1, 2, 0, 3):
                weight_copy(l, k).wait()

        @pl.when(stage(0))
        def _():
            project(l, at(0))

        @pl.when((t == 1) & (l < layers - 1))
        def _():
            for k in (1, 2, 0, 3):
                weight_copy(jnp.minimum(l + 1, layers - 1), k).start()

        @pl.when(stage(chunks + 1))
        def _():
            relay(1, l, at(chunks + 1))

        @pl.when(stage(chunks - 1))
        def _():
            attention(l, at(chunks - 1))

        @pl.when(stage(chunks - 2, chunks - SENT))
        def _():
            relay_before(l, at(chunks - 2), others(me))

        @pl.when(g == chunks + 1)
        def _():
            weight_copy(0, 3).wait()

        @pl.when(t == chunks + 1)
        def _():
            passed_on(l)

        @pl.when(stage(chunks + 1))
        def _():
            out_project(l, at(chunks + 1))

        @pl.when(stage(chunks + 3) & (l == layers - 1))
        def _():
            finish(at(chunks + 3))

        return carry

    lax.fori_loop(0, layers * period + 2, step, 0)
    for c in range(chunks):
        out_copy(c).wait()


def on_device(tp, sp_count, residual, gains, w_query, w_key, w_value, w_out, rel_bias):
    tokens, cols = residual.shape
    layers, width, _ = w_query.shape
    chunks = tokens // BLOCK
    reach = LEFT * SEG
    pairs = cols // 128
    ychips = tp // 2
    hbm = pl.BlockSpec(memory_space=pl.ANY)
    dma = pltpu.SemaphoreType.DMA
    return pl.pallas_call(
        functools.partial(kernel, tp, sp_count),
        out_shape=jax.ShapeDtypeStruct((tokens, cols), BF16),
        in_specs=[hbm] * 7,
        out_specs=hbm,
        scratch_shapes=[
            pltpu.VMEM((layers, 4, width, cols), BF16),
            pltpu.VMEM((2, layers, tp, tokens, cols), BF16),
            pltpu.VMEM((layers, tp, tokens - SENT * BLOCK, cols), BF16),
            pltpu.VMEM((layers, reach + tokens, cols), BF16),
            pltpu.VMEM((layers, reach // BLOCK + chunks, cols, BLOCK), BF16),
            pltpu.VMEM((tokens, cols), BF16),
            pltpu.VMEM((tokens, cols), F32),
            pltpu.VMEM((layers, pairs, 2, BLOCK, 2 * BLOCK), F32),
            pltpu.VMEM((chunks, tp, 8, BLOCK), F32),
            pltpu.VMEM(gains.shape, F32),
            pltpu.VMEM(rel_bias.shape, F32),
            pltpu.VMEM((tokens, cols), BF16),
            dma((layers, 4)),
            dma((chunks + 2,)),
            dma((2, chunks, tp)),
            dma((2, chunks, tp)),
            dma((2, chunks, ychips)),
            dma((chunks - SENT, ychips)),
            dma((layers, chunks - SENT, tp)),
            dma((chunks - SENT, ychips)),
            dma((SENT, 2)),
            dma((layers, SENT, 2)),
            dma((chunks, tp)),
            dma((chunks, tp)),
        ],
        compiler_params=pltpu.CompilerParams(
            collective_id=0, has_side_effects=True, vmem_limit_bytes=58 * 2**20
        ),
    )(residual, gains, rel_bias, w_query, w_key, w_value, w_out)


def solution(mesh):
    return jax.shard_map(
        functools.partial(on_device, mesh.shape["tp"], mesh.shape["sp"]),
        mesh=mesh,
        in_specs=(
            P("sp", "tp"),
            P(),
            P(None, None, "tp"),
            P(None, None, "tp"),
            P(None, None, "tp"),
            P(None, None, "tp"),
            P(None, "tp", None),
        ),
        out_specs=P("sp", "tp"),
        check_vma=False,
    )
```

time: 90.9 us -> 77.2 us (0.85)
  the two profiles are of different devices: /device:TPU:9 before, /device:TPU:0 now
where the time goes in v1:
time: 77.2 us; the launch traced here: 75.8 us
  Pallas kernels  73.9 us (96%)
  local copies, waits for them, and re-layouts  1.87 us (2%)
    pallas_call x1, Pallas kernels, on_device(): pl.pallas_call(functools.partial(kernel, tp, sp_count), out_shape=jax.Sha...  73.9 us
    unnamed x1, local copies, waits for them, and re-layouts  1.87 us

profile of v1, /device:TPU:0, one launch (start us, length us, event | category | flops | bytes accessed | tf_op | source)
XLA Modules:
  0.0 75.8 jit_solution(13218463742670517988)
XLA Ops:
  0.0 73.9 %shard_map.73 = bf16[512,512]{1,0:T(8,128)(2,1)} custom-call(bf16[512,512]{1,0:T(8,128)(2,1)} %res_ref.1, f32[2,2,2048]{2,1,0:T(2,128)} %gains_hbm.1, f32[2,8,257]{2,1,0:T(8,128)} %bias_hbm.1, bf16[2,2048,512]{2,1,0:T(8,128)(2,1)} %wq_ref.1, bf16[2,2048,512]{2,1,0:T(8,128)(2,1)} %wk_ref.1, bf16[2,2048,512]{2,1,0:T(8,128)(2,1)} %wv_ref.1, ...), custom_call_target="tpu_custom_call" | custom-call | tf_op jit(solution)/shard_map/pallas_call | solution.py:514
  73.9 1.9 %copy.9 = bf16[512,512]{1,0:T(8,128)(2,1)} copy(bf16[512,512]{1,0:T(8,128)(2,1)} %shard_map.73) | data formatting | bytes 1048576

commit v2 on v1

--- a/solution.py
+++ b/solution.py
@@ -114,11 +114,14 @@
         pl.semaphore_signal(
             barrier, inc=1, device_id={"tp": lax.rem(me + k, tp)}, device_id_type=MESH
         )
-    for k in (1, sp_count - 1):
+
+    @pl.when(~first)
+    def _():
         pl.semaphore_signal(
-            barrier, inc=1, device_id={"sp": lax.rem(sp + k, sp_count)}, device_id_type=MESH
-        )
-    pl.semaphore_wait(barrier, tp + 1)
+            barrier, inc=1, device_id={"sp": jnp.maximum(sp - 1, 0)}, device_id_type=MESH
+        )
+
+    pl.semaphore_wait(barrier, jnp.where(last, tp - 1, tp))
 
     def block_of(kind, l, c, slot):
         return gather.at[kind, l, slot, rows_of(c)]
@@ -423,29 +426,29 @@
     lax.fori_loop(0, layers, tables, 0)
     gains_copy.wait()
 
-    period = 2 * chunks + 1
+    period = 2 * chunks
 
     def step(g, carry):
-        l = jnp.minimum(g // period, layers - 1)
-        t = g - l * period
-
         def stage(lag, count=chunks):
-            return (t >= lag) & (t < lag + count)
-
-        def at(lag):
-            return chunks - 1 - t + lag
-
-        @pl.when(stage(0))
-        def _():
-            relay_stream(l, at(0))
-
-        @pl.when(stage(1, chunks - SENT))
-        def _():
-            relay_before(l, at(1), [me])
-
-        @pl.when(stage(chunks - 1, chunks - SENT))
-        def _():
-            project_before(l, at(chunks - 1))
+            index = g - lag
+            l = jnp.clip(index // period, 0, layers - 1)
+            t = index - l * period
+            return (t >= 0) & (t < count), l, chunks - 1 - t
+
+        def on(lag, count=chunks, extra=True):
+            live, l, c = stage(lag, count)
+            return lambda run: pl.when(live & extra)(lambda: run(l, c))
+
+        def layer_at(lag):
+            return jnp.clip((g - lag) // period, 0, layers - 1)
+
+        def relay_rest(l, c):
+            pl.when(c >= SENT)(lambda: relay_before(l, c, others(me)))
+
+        on(0)(relay_stream)
+        on(chunks - 2, 1)(relay_rest)
+        on(chunks - 1, 1, layer_at(chunks - 1) > 0)(lambda l, c: relay_rest(l, c - 1))
+        on(chunks - 1, chunks - SENT)(project_before)
 
         @pl.when(g == 0)
         def _():
@@ -453,51 +456,33 @@
                 weight_copy(0, k).wait()
             weight_copy(0, 3).start()
 
-        @pl.when((t == 0) & (l > 0))
+        @pl.when((g > 0) & (lax.rem(g, period) == 0) & (g < layers * period))
         def _():
             for k in (1, 2, 0, 3):
-                weight_copy(l, k).wait()
-
-        @pl.when(stage(0))
-        def _():
-            project(l, at(0))
-
-        @pl.when((t == 1) & (l < layers - 1))
+                weight_copy(layer_at(0), k).wait()
+
+        on(0)(project)
+        on(1, chunks - SENT)(lambda l, c: relay_before(l, c, [me]))
+
+        @pl.when((lax.rem(g, period) == 1) & (g < (layers - 1) * period))
         def _():
             for k in (1, 2, 0, 3):
-                weight_copy(jnp.minimum(l + 1, layers - 1), k).start()
-
-        @pl.when(stage(chunks + 1))
-        def _():
-            relay(1, l, at(chunks + 1))
-
-        @pl.when(stage(chunks - 1))
-        def _():
-            attention(l, at(chunks - 1))
-
-        @pl.when(stage(chunks - 2, chunks - SENT))
-        def _():
-            relay_before(l, at(chunks - 2), others(me))
+                weight_copy(jnp.minimum(layer_at(0) + 1, layers - 1), k).start()
+
+        on(chunks + 1)(lambda l, c: relay(1, l, c))
+        on(chunks - 1)(attention)
+        on(chunks - 1, chunks - SENT - 1)(lambda l, c: relay_rest(l, c - 1 - jnp.minimum(l, 1)))
 
         @pl.when(g == chunks + 1)
         def _():
             weight_copy(0, 3).wait()
 
-        @pl.when(t == chunks + 1)
-        def _():
-            passed_on(l)
-
-        @pl.when(stage(chunks + 1))
-        def _():
-            out_project(l, at(chunks + 1))
-
-        @pl.when(stage(chunks + 3) & (l == layers - 1))
-        def _():
-            finish(at(chunks + 3))
-
+        on(chunks + 1, 1)(lambda l, c: passed_on(l))
+        on(chunks + 1)(out_project)
+        on(chunks + 3, chunks, layer_at(chunks + 3) == layers - 1)(lambda l, c: finish(c))
         return carry
 
-    lax.fori_loop(0, layers * period + 2, step, 0)
+    lax.fori_loop(0, (layers - 1) * period + 2 * chunks + 3, step, 0)
     for c in range(chunks):
         out_copy(c).wait()
 

time: 77.2 us -> 71.5 us (0.926); the launches traced: 75.8 us -> 71.4 us
  Pallas kernels: 73.9 us -> 69.5 us
    pallas_call x1, Pallas kernels: 73.9 us -> 69.5 us  [on_device(): pl.pallas_call(functools.partial(kernel, tp, sp_count), out_shape=jax.Sha...]
where the time goes in v2:
time: 71.5 us; the launch traced here: 71.4 us
  Pallas kernels  69.5 us (97%)
  local copies, waits for them, and re-layouts  1.87 us (3%)
    pallas_call x1, Pallas kernels, on_device(): pl.pallas_call(functools.partial(kernel, tp, sp_count), out_shape=jax.Sha...  69.5 us
    unnamed x1, local copies, waits for them, and re-layouts  1.87 us

profile of v2, /device:TPU:0, one launch (start us, length us, event | category | flops | bytes accessed | tf_op | source)
XLA Modules:
  0.0 71.4 jit_solution(8336231896890469778)
XLA Ops:
  0.0 69.5 %shard_map.73 = bf16[512,512]{1,0:T(8,128)(2,1)} custom-call(bf16[512,512]{1,0:T(8,128)(2,1)} %res_ref.1, f32[2,2,2048]{2,1,0:T(2,128)} %gains_hbm.1, f32[2,8,257]{2,1,0:T(8,128)} %bias_hbm.1, bf16[2,2048,512]{2,1,0:T(8,128)(2,1)} %wq_ref.1, bf16[2,2048,512]{2,1,0:T(8,128)(2,1)} %wk_ref.1, bf16[2,2048,512]{2,1,0:T(8,128)(2,1)} %wv_ref.1, ...), custom_call_target="tpu_custom_call" | custom-call | tf_op jit(solution)/shard_map/pallas_call | solution.py:499
  69.5 1.9 %copy.9 = bf16[512,512]{1,0:T(8,128)(2,1)} copy(bf16[512,512]{1,0:T(8,128)(2,1)} %shard_map.73) | data formatting | bytes 1048576

commit v3 on v2

--- a/solution.py
+++ b/solution.py
@@ -54,7 +54,6 @@
     sums,
     gains_ref,
     bias_ref,
-    final,
     w_sem,
     io_sem,
     g_send,
@@ -96,9 +95,6 @@
             res_ref.at[rows_of(c)], gather.at[0, 0, me, rows_of(c)], io_sem.at[c]
         )
 
-    def out_copy(c):
-        return pltpu.make_async_copy(final.at[rows_of(c)], out_ref.at[rows_of(c)], io_sem.at[c])
-
     gains_copy = pltpu.make_async_copy(gains_hbm, gains_ref, io_sem.at[chunks])
     bias_copy = pltpu.make_async_copy(bias_hbm, bias_ref, io_sem.at[chunks + 1])
 
@@ -123,26 +119,27 @@
 
     pl.semaphore_wait(barrier, jnp.where(last, tp - 1, tp))
 
-    def block_of(kind, l, c, slot):
-        return gather.at[kind, l, slot, rows_of(c)]
-
-    def direct(kind, l, c, peer, source):
-        ref = block_of(kind, l, c, source)
-        return remote(ref, ref, g_send.at[kind, c, peer], g_recv.at[kind, c, source], {"tp": peer})
+    def block_of(kind, l, c, slot, lanes=slice(None)):
+        return gather.at[kind, l, slot, rows_of(c), lanes]
+
+    def direct(kind, l, c, peer, source, lanes=slice(None)):
+        ref = block_of(kind, l, c, source, lanes)
+        way = jnp.where(peer == sibling, ychips - 1, lax.rem(peer // 2 + ychips - me // 2, ychips) - 1)
+        return remote(ref, ref, g_send.at[c, way], g_recv.at[kind, c, source], {"tp": peer})
 
     def forward(kind, l, c, source):
         ref = block_of(kind, l, c, source)
         return remote(
-            ref, ref, f_send.at[kind, c, source // 2], g_recv.at[kind, c, source], {"tp": sibling}
+            ref, ref, f_send.at[c, source // 2], g_recv.at[kind, c, source], {"tp": sibling}
         )
 
     def others(base):
         return [lax.rem(base + 2 * k, tp) for k in range(1, ychips)]
 
-    def spread(kind, l, c):
+    def spread(kind, l, c, lanes=slice(None)):
         for peer in others(me):
-            direct(kind, l, c, peer, me).start()
-        direct(kind, l, c, sibling, me).start()
+            direct(kind, l, c, peer, me, lanes).start()
+        direct(kind, l, c, sibling, me, lanes).start()
 
     def relay(kind, l, c):
         for source in others(me):
@@ -185,7 +182,7 @@
             for source in others(me):
                 pass_on(l, c, source).start()
 
-        @pl.when((l == 0) & (c == chunks - 1) & ~last)
+        @pl.when((l == 0) & (c == chunks - 2) & ~last)
         def _():
             for held in reversed(range(SENT, chunks - 2)):
                 pass_on(0, held, me).start()
@@ -277,14 +274,18 @@
                 gather[0, 0, j, rows] = part
 
         scaled, inv = scaled_and_inv(l, [gather[0, 0, j, rows] for j in range(tp)])
-        query = jnp.dot(scaled, wbuf[l, 0], preferred_element_type=F32)
-        qbuf[rows_of(c)] = (query * (inv * (LOG2E * HEAD**-0.5))).astype(BF16)
         store_keys_values(l, c + blocks, scaled, inv)
 
         @pl.when((c < SENT) & ~last)
         def _():
             halo(l, c, 0).start()
             halo(l, c, 1).start()
+
+    def ask(l, c):
+        rows = rows_of(c)
+        scaled, inv = scaled_and_inv(l, [gather[0, 0, j, rows] for j in range(tp)])
+        query = jnp.dot(scaled, wbuf[l, 0], preferred_element_type=F32)
+        qbuf[rows] = (query * (inv * (LOG2E * HEAD**-0.5))).astype(BF16)
 
     def project_before(l, c):
         @pl.when(~first)
@@ -361,30 +362,31 @@
         held = [score(pair) for pair in range(pairs)]
         for pair in range(pairs):
             mix(pair, *held[pair])
-        spread(1, l, c)
-
-    def out_project(l, c):
+            if pair == pairs // 2 - 1:
+                spread(1, l, c, slice(0, (pair + 1) * 128))
+        spread(1, l, c, slice(pairs // 2 * 128, cols))
+
+    def out_product(l, c):
         arrive(1, l, c)
         whole = jnp.concatenate([gather[1, l, j, rows_of(c)] for j in range(tp)], axis=1)
-        value = jnp.dot(whole, wbuf[l, 3], preferred_element_type=F32)
-
-        @pl.when(l < layers - 1)
-        def _():
-            later = jnp.minimum(l + 1, layers - 1)
-            gather[0, later, me, rows_of(c)] = value.astype(BF16)
-            spread(0, later, c)
-
-            @pl.when((c >= SENT) & ~last)
-            def _():
-                pass_on(later, c, me).start()
-
-        @pl.when(l == layers - 1)
-        def _():
-            branch[rows_of(c)] = value
-            square = jnp.sum(value * value, axis=1, keepdims=True)
-            sums[c, me] = jnp.broadcast_to(square, (BLOCK, BLOCK)).T[:8]
-            for k in range(1, tp):
-                sum_copy(c, lax.rem(me + k, tp), me).start()
+        return jnp.dot(whole, wbuf[l, 3], preferred_element_type=F32)
+
+    def hand_on(l, c):
+        later = jnp.minimum(l + 1, layers - 1)
+        gather[0, later, me, rows_of(c)] = out_product(l, c).astype(BF16)
+        spread(0, later, c)
+
+        @pl.when((c >= SENT) & ~last)
+        def _():
+            pass_on(later, c, me).start()
+
+    def out_project(l, c):
+        value = out_product(l, c)
+        branch[rows_of(c)] = value
+        square = jnp.sum(value * value, axis=1, keepdims=True)
+        sums[c, me] = jnp.broadcast_to(square, (BLOCK, BLOCK)).T[:8]
+        for k in range(1, tp):
+            sum_copy(c, lax.rem(me + k, tp), me).start()
 
     def finish(c):
         for k in range(1, tp):
@@ -396,8 +398,7 @@
         inv = jnp.broadcast_to(inv[0:1], (BLOCK, BLOCK)).T[:, 0:1]
         gain = gains_ref[layers - 1, 1:2, pl.ds(pl.multiple_of(me * cols, 128), cols)]
         new = gather[0, 0, me, rows_of(c)].astype(F32) + branch[rows_of(c)] * inv * gain
-        final[rows_of(c)] = new.astype(BF16)
-        out_copy(c).start()
+        out_ref[rows_of(c)] = new.astype(BF16)
 
     def passed_on(l):
         @pl.when(~last)
@@ -426,6 +427,10 @@
     lax.fori_loop(0, layers, tables, 0)
     gains_copy.wait()
 
+    def closing(t, carry):
+        finish(chunks - 1 - t)
+        return carry
+
     period = 2 * chunks
 
     def step(g, carry):
@@ -443,11 +448,11 @@
             return jnp.clip((g - lag) // period, 0, layers - 1)
 
         def relay_rest(l, c):
+            pl.when((c >= SENT) & (c < chunks - 2))(lambda: relay_before(l, c, [me]))
             pl.when(c >= SENT)(lambda: relay_before(l, c, others(me)))
 
         on(0)(relay_stream)
         on(chunks - 2, 1)(relay_rest)
-        on(chunks - 1, 1, layer_at(chunks - 1) > 0)(lambda l, c: relay_rest(l, c - 1))
         on(chunks - 1, chunks - SENT)(project_before)
 
         @pl.when(g == 0)
@@ -461,30 +466,34 @@
             for k in (1, 2, 0, 3):
                 weight_copy(layer_at(0), k).wait()
 
+        on(1, chunks - 2)(ask)
         on(0)(project)
-        on(1, chunks - SENT)(lambda l, c: relay_before(l, c, [me]))
+        on(1, 2)(lambda l, c: relay_before(l, c, [me]))
+        on(chunks - 1, 1)(lambda l, c: relay_rest(l, c - 1))
 
         @pl.when((lax.rem(g, period) == 1) & (g < (layers - 1) * period))
         def _():
             for k in (1, 2, 0, 3):
                 weight_copy(jnp.minimum(layer_at(0) + 1, layers - 1), k).start()
 
-        on(chunks + 1)(lambda l, c: relay(1, l, c))
+        on(chunks + 1, chunks, layer_at(chunks + 1) < layers - 1)(lambda l, c: relay(1, l, c))
+        on(chunks + 2, chunks, layer_at(chunks + 2) == layers - 1)(lambda l, c: relay(1, l, c))
         on(chunks - 1)(attention)
-        on(chunks - 1, chunks - SENT - 1)(lambda l, c: relay_rest(l, c - 1 - jnp.minimum(l, 1)))
+        on(chunks, 2)(lambda l, c: ask(l, c - chunks + 2))
+        on(chunks - 1, chunks - SENT - 2, layer_at(chunks - 1) > 0)(lambda l, c: relay_rest(l, c - 2))
+        on(chunks, chunks - SENT - 2, layer_at(chunks) == 0)(lambda l, c: relay_rest(l, c - 2))
 
         @pl.when(g == chunks + 1)
         def _():
             weight_copy(0, 3).wait()
 
         on(chunks + 1, 1)(lambda l, c: passed_on(l))
-        on(chunks + 1)(out_project)
-        on(chunks + 3, chunks, layer_at(chunks + 3) == layers - 1)(lambda l, c: finish(c))
+        on(chunks + 1, chunks, layer_at(chunks + 1) < layers - 1)(hand_on)
+        on(chunks + 2, chunks, layer_at(chunks + 2) == layers - 1)(out_project)
         return carry
 
-    lax.fori_loop(0, (layers - 1) * period + 2 * chunks + 3, step, 0)
-    for c in range(chunks):
-        out_copy(c).wait()
+    lax.fori_loop(0, (layers - 1) * period + 2 * chunks + 2, step, 0)
+    lax.fori_loop(0, chunks, closing, 0)
 
 
 def on_device(tp, sp_count, residual, gains, w_query, w_key, w_value, w_out, rel_bias):
@@ -496,11 +505,11 @@
     ychips = tp // 2
     hbm = pl.BlockSpec(memory_space=pl.ANY)
     dma = pltpu.SemaphoreType.DMA
-    return pl.pallas_call(
+    staged = pl.pallas_call(
         functools.partial(kernel, tp, sp_count),
-        out_shape=jax.ShapeDtypeStruct((tokens, cols), BF16),
+        out_shape=pltpu.VMEM((tokens, cols), BF16),
         in_specs=[hbm] * 7,
-        out_specs=hbm,
+        out_specs=pl.BlockSpec(memory_space=pltpu.VMEM),
         scratch_shapes=[
             pltpu.VMEM((layers, 4, width, cols), BF16),
             pltpu.VMEM((2, layers, tp, tokens, cols), BF16),
@@ -513,12 +522,11 @@
             pltpu.VMEM((chunks, tp, 8, BLOCK), F32),
             pltpu.VMEM(gains.shape, F32),
             pltpu.VMEM(rel_bias.shape, F32),
-            pltpu.VMEM((tokens, cols), BF16),
             dma((layers, 4)),
             dma((chunks + 2,)),
+            dma((chunks, ychips)),
             dma((2, chunks, tp)),
-            dma((2, chunks, tp)),
-            dma((2, chunks, ychips)),
+            dma((chunks, ychips)),
             dma((chunks - SENT, ychips)),
             dma((layers, chunks - SENT, tp)),
             dma((chunks - SENT, ychips)),
@@ -531,6 +539,7 @@
             collective_id=0, has_side_effects=True, vmem_limit_bytes=58 * 2**20
         ),
     )(residual, gains, rel_bias, w_query, w_key, w_value, w_out)
+    return staged
 
 
 def solution(mesh):

time: 71.5 us -> 67.5 us (0.944)
  Pallas kernels: 69.5 us -> 66.5 us
  local copies, waits for them, and re-layouts: 1.87 us -> 0.8 us
    pallas_call x1, Pallas kernels: 69.5 us -> 66.5 us  [on_device(): pl.pallas_call(functools.partial(kernel, tp, sp_count), out_shape=pltpu.V...]
    unnamed x1, local copies, waits for them, and re-layouts: 1.87 us -> 0.8 us
where the time goes in v3:
time: 67.5 us; the launch traced here: 67.4 us
  Pallas kernels  66.5 us (99%)
  local copies, waits for them, and re-layouts  0.8 us (1%)
    pallas_call x1, Pallas kernels, on_device(): pl.pallas_call(functools.partial(kernel, tp, sp_count), out_shape=pltpu.V...  66.5 us

profile of v3, /device:TPU:0, one launch (start us, length us, event | category | flops | bytes accessed | tf_op | source)
XLA Modules:
  0.0 67.4 jit_solution(10373548026821481589)
XLA Ops:
  0.0 66.5 %shard_map.73 = bf16[512,512]{1,0:T(8,128)(2,1)S(1)} custom-call(bf16[512,512]{1,0:T(8,128)(2,1)} %res_ref.1, f32[2,2,2048]{2,1,0:T(2,128)} %gains_hbm.1, f32[2,8,257]{2,1,0:T(8,128)} %bias_hbm.1, bf16[2,2048,512]{2,1,0:T(8,128)(2,1)} %wq_ref.1, bf16[2,2048,512]{2,1,0:T(8,128)(2,1)} %wk_ref.1, bf16[2,2048,512]{2,1,0:T(8,128)(2,1)} %wv_ref.1, ...), custom_call_target="tpu_custom_call" | custom-call | tf_op jit(solution)/shard_map/pallas_call | solution.py:508
  66.6 0.8 %copy.9 = bf16[512,512]{1,0:T(8,128)(2,1)} copy(bf16[512,512]{1,0:T(8,128)(2,1)S(1)} %shard_map.73) | data formatting | bytes 1048576

commit v4 on v3

--- a/solution.py
+++ b/solution.py
@@ -64,8 +64,6 @@
     bf_send,
     h_send,
     h_recv,
-    s_send,
-    s_recv,
 ):
     layers = wbuf.shape[0]
     tokens, cols = res_ref.shape
@@ -182,10 +180,10 @@
             for source in others(me):
                 pass_on(l, c, source).start()
 
-        @pl.when((l == 0) & (c == chunks - 2) & ~last)
+        @pl.when((c == jnp.where(l == 0, chunks - 2, chunks - 1)) & ~last)
         def _():
             for held in reversed(range(SENT, chunks - 2)):
-                pass_on(0, held, me).start()
+                pass_on(l, held, me).start()
 
     def update(l, parts):
         old, branches = parts
@@ -218,9 +216,16 @@
             {"sp": lax.rem(sp + 1, sp_count)},
         )
 
-    def sum_copy(c, peer, source):
-        ref = sums.at[c, source]
-        return remote(ref, ref, s_send.at[c, peer], s_recv.at[c, source], {"tp": peer})
+    def sum_copies(c):
+        pairs_of = [(peer, g_send.at[c, k]) for k, peer in enumerate(others(me))]
+        pairs_of.append((sibling, g_send.at[c, ychips - 1]))
+        pairs_of += [(peer, f_send.at[c, k]) for k, peer in enumerate(others(sibling))]
+
+        def copy(peer, source, sem):
+            ref = sums.at[c, source]
+            return remote(ref, ref, sem, g_recv.at[0, c, source], {"tp": peer})
+
+        return [(copy(peer, me, sem), copy(peer, peer, sem)) for peer, sem in pairs_of]
 
     for c in reversed(range(chunks)):
         res_copy(c).wait()
@@ -376,7 +381,7 @@
         gather[0, later, me, rows_of(c)] = out_product(l, c).astype(BF16)
         spread(0, later, c)
 
-        @pl.when((c >= SENT) & ~last)
+        @pl.when((c >= max(SENT, chunks - 2)) & ~last)
         def _():
             pass_on(later, c, me).start()
 
@@ -385,14 +390,13 @@
         branch[rows_of(c)] = value
         square = jnp.sum(value * value, axis=1, keepdims=True)
         sums[c, me] = jnp.broadcast_to(square, (BLOCK, BLOCK)).T[:8]
-        for k in range(1, tp):
-            sum_copy(c, lax.rem(me + k, tp), me).start()
+        for mine, _ in sum_copies(c):
+            mine.start()
 
     def finish(c):
-        for k in range(1, tp):
-            peer = lax.rem(me + k, tp)
-            sum_copy(c, peer, peer).wait_recv()
-            sum_copy(c, peer, me).wait_send()
+        for mine, theirs in sum_copies(c):
+            theirs.wait_recv()
+            mine.wait_send()
         total = functools.reduce(jnp.add, [sums[c, j] for j in range(tp)])
         inv = lax.rsqrt(total / width + EPS)
         inv = jnp.broadcast_to(inv[0:1], (BLOCK, BLOCK)).T[:, 0:1]
@@ -452,8 +456,17 @@
             pl.when(c >= SENT)(lambda: relay_before(l, c, others(me)))
 
         on(0)(relay_stream)
-        on(chunks - 2, 1)(relay_rest)
-        on(chunks - 1, chunks - SENT)(project_before)
+        on(1, 2)(lambda l, c: relay_before(l, c, [me]))
+        live, l, c = stage(1, 2)
+        pl.when(live & (c == jnp.where(l == 0, chunks - 2, chunks - 1)))(
+            lambda: relay_rest(l, chunks - 1)
+        )
+        before_live, before_l, c = stage(chunks - 2, chunks - SENT + 1)
+        u = chunks - 1 - c
+        before_c = jnp.where(u == 0, chunks - 1, chunks - u)
+        pl.when(before_live & (u != jnp.where(before_l == 0, 0, 1)))(
+            lambda: project_before(before_l, before_c)
+        )
 
         @pl.when(g == 0)
         def _():
@@ -466,9 +479,20 @@
             for k in (1, 2, 0, 3):
                 weight_copy(layer_at(0), k).wait()
 
-        on(1, chunks - 2)(ask)
+        ask_live, ask_l, c = stage(1, 3)
+        v = chunks - 1 - c
+
+        @pl.when(ask_live & ((v == 0) | (v == jnp.where(ask_l == 0, 1, 2))))
+        def _():
+            first_c = chunks - 1 - jnp.minimum(v, 1)
+
+            def one(i, carry):
+                ask(ask_l, first_c - i)
+                return carry
+
+            lax.fori_loop(0, jnp.where(v == 2, 2, 1), one, 0)
+
         on(0)(project)
-        on(1, 2)(lambda l, c: relay_before(l, c, [me]))
         on(chunks - 1, 1)(lambda l, c: relay_rest(l, c - 1))
 
         @pl.when((lax.rem(g, period) == 1) & (g < (layers - 1) * period))
@@ -479,7 +503,10 @@
         on(chunks + 1, chunks, layer_at(chunks + 1) < layers - 1)(lambda l, c: relay(1, l, c))
         on(chunks + 2, chunks, layer_at(chunks + 2) == layers - 1)(lambda l, c: relay(1, l, c))
         on(chunks - 1)(attention)
-        on(chunks, 2)(lambda l, c: ask(l, c - chunks + 2))
+        rest_live, rest_l, rest_c = stage(chunks, 2)
+        pl.when(rest_live & ((rest_l == 0) | (rest_c == chunks - 2)))(
+            lambda: ask(rest_l, rest_c - chunks + 2)
+        )
         on(chunks - 1, chunks - SENT - 2, layer_at(chunks - 1) > 0)(lambda l, c: relay_rest(l, c - 2))
         on(chunks, chunks - SENT - 2, layer_at(chunks) == 0)(lambda l, c: relay_rest(l, c - 2))
 
@@ -532,8 +559,6 @@
             dma((chunks - SENT, ychips)),
             dma((SENT, 2)),
             dma((layers, SENT, 2)),
-            dma((chunks, tp)),
-            dma((chunks, tp)),
         ],
         compiler_params=pltpu.CompilerParams(
             collective_id=0, has_side_effects=True, vmem_limit_bytes=58 * 2**20

time: 67.5 us -> 67.3 us (level)
  no operation moved by 1% of the time
where the time goes in v4:
time: 67.3 us; the launch traced here: 67.1 us
  Pallas kernels  66.3 us (99%)
  local copies, waits for them, and re-layouts  0.8 us (1%)
    pallas_call x1, Pallas kernels, on_device(): pl.pallas_call(functools.partial(kernel, tp, sp_count), out_shape=pltpu.V...  66.3 us

profile of v4, /device:TPU:0, one launch (start us, length us, event | category | flops | bytes accessed | tf_op | source)
XLA Modules:
  0.0 67.1 jit_solution(15177951452424404050)
XLA Ops:
  0.0 66.3 %shard_map.73 = bf16[512,512]{1,0:T(8,128)(2,1)S(1)} custom-call(bf16[512,512]{1,0:T(8,128)(2,1)} %res_ref.1, f32[2,2,2048]{2,1,0:T(2,128)} %gains_hbm.1, f32[2,8,257]{2,1,0:T(8,128)} %bias_hbm.1, bf16[2,2048,512]{2,1,0:T(8,128)(2,1)} %wq_ref.1, bf16[2,2048,512]{2,1,0:T(8,128)(2,1)} %wk_ref.1, bf16[2,2048,512]{2,1,0:T(8,128)(2,1)} %wv_ref.1, ...), custom_call_target="tpu_custom_call" | custom-call | tf_op jit(solution)/shard_map/pallas_call | solution.py:535
  66.3 0.8 %copy.9 = bf16[512,512]{1,0:T(8,128)(2,1)} copy(bf16[512,512]{1,0:T(8,128)(2,1)S(1)} %shard_map.73) | data formatting | bytes 1048576

commit v5 on v4

--- a/solution.py
+++ b/solution.py
@@ -148,6 +148,9 @@
         direct(kind, l, c, sibling, sibling).wait_recv()
         for source in others(sibling):
             direct(kind, l, c, sibling, source).wait_recv()
+        sent(kind, l, c)
+
+    def sent(kind, l, c):
         for source in others(me):
             forward(kind, l, c, source).wait_send()
             direct(kind, l, c, source, me).wait_send()
@@ -263,10 +266,10 @@
         return scaled, lax.rsqrt(total / width + EPS)
 
     def store_keys_values(l, slot, scaled, inv):
+        value = jnp.dot(scaled, wbuf[l, 2], preferred_element_type=F32)
+        vbuf[l, slot] = (value * inv).T.astype(BF16)
         key = jnp.dot(scaled, wbuf[l, 1], preferred_element_type=F32)
         kbuf[l, rows_of(slot)] = (key * inv).astype(BF16)
-        value = jnp.dot(scaled, wbuf[l, 2], preferred_element_type=F32)
-        vbuf[l, slot] = (value * inv).T.astype(BF16)
 
     def project(l, c):
         arrive(0, l, c)
@@ -275,11 +278,15 @@
         @pl.when(l > 0)
         def _():
             own = ([gather[0, k, j, rows] for j in range(tp)] for k in (0, l))
-            for j, part in enumerate(update(l, own)):
+            parts = update(l, own)
+            for j, part in enumerate(parts):
                 gather[0, 0, j, rows] = part
-
-        scaled, inv = scaled_and_inv(l, [gather[0, 0, j, rows] for j in range(tp)])
-        store_keys_values(l, c + blocks, scaled, inv)
+            store_keys_values(l, c + blocks, *scaled_and_inv(l, parts))
+
+        @pl.when(l == 0)
+        def _():
+            parts = [gather[0, 0, j, rows] for j in range(tp)]
+            store_keys_values(l, c + blocks, *scaled_and_inv(l, parts))
 
         @pl.when((c < SENT) & ~last)
         def _():
@@ -304,11 +311,15 @@
             @pl.when(l > 0)
             def _():
                 halo_parts = ([before[k, j, rows] for j in range(tp)] for k in (0, l))
-                for j, part in enumerate(update(l, halo_parts)):
+                parts = update(l, halo_parts)
+                for j, part in enumerate(parts):
                     before[0, j, rows] = part
-
-            scaled, inv = scaled_and_inv(l, [before[0, j, rows] for j in range(tp)])
-            store_keys_values(l, c, scaled, inv)
+                store_keys_values(l, c, *scaled_and_inv(l, parts))
+
+            @pl.when(l == 0)
+            def _():
+                parts = [before[0, j, rows] for j in range(tp)]
+                store_keys_values(l, c, *scaled_and_inv(l, parts))
 
     def attention(l, c):
         @pl.when((c < SENT) & ~first)
@@ -386,7 +397,24 @@
             pass_on(later, c, me).start()
 
     def out_project(l, c):
-        value = out_product(l, c)
+        def product(sources):
+            total = None
+            for source in sources:
+                rows = pl.ds(pl.multiple_of(source * cols, cols), cols)
+                part = jnp.dot(
+                    gather[1, l, source, rows_of(c)],
+                    wbuf[l, 3, rows],
+                    preferred_element_type=F32,
+                )
+                total = part if total is None else total + part
+            return total
+
+        direct(1, l, c, sibling, sibling).wait_recv()
+        branch[rows_of(c)] = product([me, sibling] + others(me))
+        for source in others(sibling):
+            direct(1, l, c, sibling, source).wait_recv()
+        sent(1, l, c)
+        value = branch[rows_of(c)] + product(others(sibling))
         branch[rows_of(c)] = value
         square = jnp.sum(value * value, axis=1, keepdims=True)
         sums[c, me] = jnp.broadcast_to(square, (BLOCK, BLOCK)).T[:8]

time: 67.3 us -> 66.7 us (level)
  no operation moved by 1% of the time
where the time goes in v5:
time: 66.7 us; the launch traced here: 66.5 us
  Pallas kernels  65.7 us (99%)
  local copies, waits for them, and re-layouts  0.8 us (1%)
    pallas_call x1, Pallas kernels, on_device(): pl.pallas_call(functools.partial(kernel, tp, sp_count), out_shape=pltpu.V...  65.7 us

profile of v5, /device:TPU:0, one launch (start us, length us, event | category | flops | bytes accessed | tf_op | source)
XLA Modules:
  0.0 66.5 jit_solution(17870993121903109417)
XLA Ops:
  0.0 65.7 %shard_map.73 = bf16[512,512]{1,0:T(8,128)(2,1)S(1)} custom-call(bf16[512,512]{1,0:T(8,128)(2,1)} %res_ref.1, f32[2,2,2048]{2,1,0:T(2,128)} %gains_hbm.1, f32[2,8,257]{2,1,0:T(8,128)} %bias_hbm.1, bf16[2,2048,512]{2,1,0:T(8,128)(2,1)} %wq_ref.1, bf16[2,2048,512]{2,1,0:T(8,128)(2,1)} %wk_ref.1, bf16[2,2048,512]{2,1,0:T(8,128)(2,1)} %wv_ref.1, ...), custom_call_target="tpu_custom_call" | custom-call | tf_op jit(solution)/shard_map/pallas_call | solution.py:563
  65.7 0.8 %copy.9 = bf16[512,512]{1,0:T(8,128)(2,1)} copy(bf16[512,512]{1,0:T(8,128)(2,1)S(1)} %shard_map.73) | data formatting | bytes 1048576

commit v6 on v5

--- a/solution.py
+++ b/solution.py
@@ -54,6 +54,8 @@
     sums,
     gains_ref,
     bias_ref,
+    held_sum,
+    held_value,
     w_sem,
     io_sem,
     g_send,
@@ -271,9 +273,39 @@
         key = jnp.dot(scaled, wbuf[l, 1], preferred_element_type=F32)
         kbuf[l, rows_of(slot)] = (key * inv).astype(BF16)
 
+    def partial_keys_values(c, sources):
+        sums_of = values = keys = None
+        for source in sources:
+            part = gather[0, 0, source, rows_of(c)].astype(F32)
+            at = pl.ds(pl.multiple_of(source * cols, cols), cols)
+            scaled = (part * gains_ref[0, 0:1, at]).astype(BF16)
+            square = jnp.sum(part * part, axis=1, keepdims=True)
+            value = jnp.dot(scaled, wbuf[0, 2, at], preferred_element_type=F32)
+            key = jnp.dot(scaled, wbuf[0, 1, at], preferred_element_type=F32)
+            sums_of = square if sums_of is None else sums_of + square
+            values = value if values is None else values + value
+            keys = key if keys is None else keys + key
+        return sums_of, values, keys
+
     def project(l, c):
-        arrive(0, l, c)
         rows = rows_of(c)
+
+        @pl.when(l == 0)
+        def _():
+            direct(0, 0, c, sibling, sibling).wait_recv()
+            square, values, keys = partial_keys_values(c, [me, sibling] + others(me))
+            held_sum[...] = jnp.broadcast_to(square, held_sum.shape)
+            held_value[0] = values
+            held_value[1] = keys
+            for source in others(sibling):
+                direct(0, 0, c, sibling, source).wait_recv()
+            sent(0, 0, c)
+            square, values, keys = partial_keys_values(c, others(sibling))
+            inv = lax.rsqrt((held_sum[:, 0:1] + square) / width + EPS)
+            vbuf[0, c + blocks] = ((held_value[0] + values) * inv).T.astype(BF16)
+            kbuf[0, rows_of(c + blocks)] = ((held_value[1] + keys) * inv).astype(BF16)
+
+        pl.when(l > 0)(lambda: arrive(0, l, c))
 
         @pl.when(l > 0)
         def _():
@@ -283,10 +315,6 @@
                 gather[0, 0, j, rows] = part
             store_keys_values(l, c + blocks, *scaled_and_inv(l, parts))
 
-        @pl.when(l == 0)
-        def _():
-            parts = [gather[0, 0, j, rows] for j in range(tp)]
-            store_keys_values(l, c + blocks, *scaled_and_inv(l, parts))
 
         @pl.when((c < SENT) & ~last)
         def _():
@@ -528,9 +556,9 @@
             for k in (1, 2, 0, 3):
                 weight_copy(jnp.minimum(layer_at(0) + 1, layers - 1), k).start()
 
-        on(chunks + 1, chunks, layer_at(chunks + 1) < layers - 1)(lambda l, c: relay(1, l, c))
         on(chunks + 2, chunks, layer_at(chunks + 2) == layers - 1)(lambda l, c: relay(1, l, c))
         on(chunks - 1)(attention)
+        on(chunks + 1, chunks, layer_at(chunks + 1) < layers - 1)(lambda l, c: relay(1, l, c))
         rest_live, rest_l, rest_c = stage(chunks, 2)
         pl.when(rest_live & ((rest_l == 0) | (rest_c == chunks - 2)))(
             lambda: ask(rest_l, rest_c - chunks + 2)
@@ -577,6 +605,8 @@
             pltpu.VMEM((chunks, tp, 8, BLOCK), F32),
             pltpu.VMEM(gains.shape, F32),
             pltpu.VMEM(rel_bias.shape, F32),
+            pltpu.VMEM((BLOCK, 128), F32),
+            pltpu.VMEM((2, BLOCK, cols), F32),
             dma((layers, 4)),
             dma((chunks + 2,)),
             dma((chunks, ychips)),

time: 66.7 us -> 66.5 us (level); the launches traced: 66.5 us -> 65.6 us
  Pallas kernels: 65.7 us -> 64.8 us
    pallas_call x1, Pallas kernels: 65.7 us -> 64.8 us  [on_device(): pl.pallas_call(functools.partial(kernel, tp, sp_count), out_shape=pltpu.V...]
where the time goes in v6:
time: 66.5 us; the launch traced here: 65.6 us
  Pallas kernels  64.8 us (97%)
  local copies, waits for them, and re-layouts  0.8 us (1%)
    pallas_call x1, Pallas kernels, on_device(): pl.pallas_call(functools.partial(kernel, tp, sp_count), out_shape=pltpu.V...  64.8 us

profile of v6, /device:TPU:0, one launch (start us, length us, event | category | flops | bytes accessed | tf_op | source)
XLA Modules:
  0.0 65.6 jit_solution(2420189280642064905)
XLA Ops:
  0.0 64.8 %shard_map.73 = bf16[512,512]{1,0:T(8,128)(2,1)S(1)} custom-call(bf16[512,512]{1,0:T(8,128)(2,1)} %res_ref.1, f32[2,2,2048]{2,1,0:T(2,128)} %gains_hbm.1, f32[2,8,257]{2,1,0:T(8,128)} %bias_hbm.1, bf16[2,2048,512]{2,1,0:T(8,128)(2,1)} %wq_ref.1, bf16[2,2048,512]{2,1,0:T(8,128)(2,1)} %wk_ref.1, bf16[2,2048,512]{2,1,0:T(8,128)(2,1)} %wv_ref.1, ...), custom_call_target="tpu_custom_call" | custom-call | tf_op jit(solution)/shard_map/pallas_call | solution.py:591
  64.8 0.8 %copy.9 = bf16[512,512]{1,0:T(8,128)(2,1)} copy(bf16[512,512]{1,0:T(8,128)(2,1)S(1)} %shard_map.73) | data formatting | bytes 1048576
